TPU v7x, 32 devices: a whole 2x2x4 slice. The times are simulated.
32 devices in a mesh: fs: 8 (over z, y), tp: 4 (over x, core).
Axes of the slice: x: 2, y: 2, z: 4, core: 2. Of those that a mesh axis runs over, the one named last changes fastest.
Arguments:
- tokens: bfloat16 [3072, 2048], P(('fs', 'tp')), may hold values from -6 to 6
- ffn1_gain: float32 [2048], replicated, may hold values from 0.1 to 1.9
- ffn1_gate: bfloat16 [2048, 5632], P('fs', 'tp'), may hold values from -0.125 to 0.125
- ffn1_up: bfloat16 [2048, 5632], P('fs', 'tp'), may hold values from -0.125 to 0.125
- ffn1_down: bfloat16 [5632, 2048], P('tp', 'fs'), may hold values from -0.078125 to 0.078125
- mix_gain: float32 [2048], replicated, may hold values from 0.1 to 1.9
- lru_in_weight: bfloat16 [2048, 1536], P('fs', 'tp'), may hold values from -0.125 to 0.125
- lru_gate_weight: bfloat16 [2048, 1536], P('fs', 'tp'), may hold values from -0.125 to 0.125
- conv_weight: bfloat16 [4, 1536], P(None, 'tp'), may hold values from -3 to 3
- gate_a_weight: bfloat16 [24, 64, 64], P('tp'), may hold values from -0.75 to 0.75
- gate_x_weight: bfloat16 [24, 64, 64], P('tp'), may hold values from -0.75 to 0.75
- decay_param: float32 [1536], P('tp'), may hold values from 3.7 to 9
- mix_out_weight: bfloat16 [1536, 2048], P('tp', 'fs'), may hold values from -0.15625 to 0.15625
- ffn2_gain: float32 [2048], replicated, may hold values from 0.1 to 1.9
- ffn2_gate: bfloat16 [2048, 5632], P('fs', 'tp'), may hold values from -0.125 to 0.125
- ffn2_up: bfloat16 [2048, 5632], P('fs', 'tp'), may hold values from -0.125 to 0.125
- ffn2_down: bfloat16 [5632, 2048], P('tp', 'fs'), may hold values from -0.078125 to 0.078125
Outputs:
- layer_out: bfloat16 [3072, 2048], P(('fs', 'tp'))
All inputs are finite; a program needn't handle non-finite values.
Results may differ from a plain program's by a relative error of at most 0.017.
Values may be sent and summed in bfloat16 or wider, within the bound.
A program may use at most 64 MiB of HBM per device.

v0:
```python
import functools
import math

import jax
import jax.numpy as jnp
from jax import lax
from jax.experimental import pallas as pl
from jax.experimental.pallas import tpu as pltpu
from jax.sharding import PartitionSpec as P

EPS = 1e-06
CORES = 2
PAIR = 2
MATS = 3
MESH = pl.DeviceIdType.MESH


def dot_nt(a, b):
    return lax.dot_general(a, b, (((1,), (1,)), ((), ())), preferred_element_type=jnp.float32)


def sigmoid(v):
    return 1.0 / (1.0 + jnp.exp(-v))


def shift_down(values, step, fill):
    pad = jnp.full((step, values.shape[1]), fill, values.dtype)
    return jnp.concatenate([pad, values[: values.shape[0] - step]], axis=0)


class Place:
    def __init__(self, n, t):
        self.n, self.t = n, t
        self.ny = math.isqrt(n // PAIR)
        self.nz = n // self.ny
        self.nq = self.nz // PAIR
        self.nx = t // CORES
        fs, tp = lax.axis_index("fs"), lax.axis_index("tp")
        self.fs, self.tp = fs, tp
        self.z, self.y = fs // self.ny, fs % self.ny
        self.q, self.zp = self.z // PAIR, self.z % PAIR
        self.x, self.c = tp // CORES, tp % CORES
        self.chips = PAIR * self.nx

    def z_at(self, i):
        q = (self.q + i // PAIR) % self.nq
        return q * PAIR + (self.zp + i % PAIR) % PAIR

    def f_at(self, i, j):
        return self.z_at(i) * self.ny + (self.y + j) % self.ny

    def at_z(self, z):
        return (z * self.ny + self.y, self.tp)

    def at_y(self, j):
        return (self.z * self.ny + (self.y + j) % self.ny, self.tp)

    def at_x(self, s):
        return (self.fs, ((self.x + s) % self.nx) * CORES + self.c)

    def other_z(self):
        return self.at_z(self.q * PAIR + 1 - self.zp)

    def other_core(self):
        return (self.fs, self.x * CORES + 1 - self.c)


def remote(src, dst, send, recv, device):
    return pltpu.make_async_remote_copy(
        src_ref=src, dst_ref=dst, send_sem=send, recv_sem=recv, device_id=device, device_id_type=MESH
    )


def layer_kernel(n, t, *refs):
    (tokens, gain1, gainm, gain2, taps, gate_a, gate_x, slope) = refs[:8]
    sources = (refs[8:11], refs[11:14], refs[14:17])
    out = refs[17]
    (w1, wm, w2, rows_of, xs, xr, ys, yr, zs, zr, own, part, hid, acc, hid_m, acc_m, res) = refs[18:35]
    (rw, zsend, ysend, lsem, gr, gs, xss, xsr, yss, ysr, zss, zsr) = refs[35:]
    weights = (w1, wm, w2)
    me = Place(n, t)
    r, dn = tokens.shape[1], tokens.shape[2]
    width = n * dn
    chips, nx, ny, nz = me.chips, me.nx, me.ny, me.nz
    mine = me.zp * nx + me.x
    rest = (1 - me.zp) * nx + me.x

    barrier = pltpu.get_barrier_semaphore()
    peers = [me.at_z((me.z + d) % nz) for d in range(1, nz)]
    peers += [me.at_y(j) for j in range(1, ny)]
    peers += [me.at_x(s) for s in range(1, nx)]
    peers += [me.other_core()]
    for peer in peers:
        pl.semaphore_signal(barrier, inc=1, device_id=peer, device_id_type=MESH)
    pl.semaphore_wait(barrier, len(peers))

    def z_piece(s, k, i):
        z = me.z_at(i)
        return remote(
            sources[s][k].at[z % PAIR],
            weights[s].at[k, me.fs],
            zsend.at[s, k, i],
            rw.at[s, k, me.fs],
            me.at_z(z),
        )

    def y_piece(s, k, i, j):
        f = me.f_at(i, 0)
        src = sources[s][k].at[me.zp] if isinstance(i, int) and i == 0 else weights[s].at[k, f]
        return remote(
            src, weights[s].at[k, f], ysend.at[s, k, i, j], rw.at[s, k, f], me.at_y(j)
        )

    def local_piece(s, k):
        return pltpu.make_async_copy(
            sources[s][k].at[me.zp], weights[s].at[k, me.fs], lsem.at[s, k]
        )

    def arrived(s, k, f):
        place = weights[s].at[k, f]
        remote(place, place, zsend.at[s, k, 0], rw.at[s, k, f], me.at_y(0)).wait_recv()

    def send_weights(s, k):
        for i in list(range(PAIR, nz)) + [1]:
            z_piece(s, k, i).start()
        for j in range(1, ny):
            y_piece(s, k, 0, j).start()
        local_piece(s, k).start()

    def forward(s, k, i):
        arrived(s, k, me.f_at(i, 0))
        for j in range(1, ny):
            y_piece(s, k, i, j).start()

    def collect(s, k):
        for i in range(nz):
            for j in range(1, ny):
                arrived(s, k, me.f_at(i, j))
        local_piece(s, k).wait()

    def row_block(g, p, c):
        return rows_of.at[g, p, c]

    def row_copy(g, p, c, slot, device):
        block = row_block(g, p, c)
        return remote(block, block, gs.at[g, slot], gr.at[g, p, c], device)

    def row_wait(g, p, c):
        block = row_block(g, p, c)
        remote(block, block, gs.at[g, 0], gr.at[g, p, c], me.other_core()).wait_recv()

    def norm_rows(values, gain):
        total = jnp.zeros((r, 1), jnp.float32)
        for f in range(n):
            wide = values(f)
            total += jnp.sum(wide * wide, axis=-1, keepdims=True)
        scale = lax.rsqrt(total / width + EPS)
        return lambda f: (values(f) * scale * gain[f]).astype(jnp.bfloat16)

    row_sends = []

    def send_rows(g, values, gain):
        normed = norm_rows(values, gain)
        for f in range(n):
            rows_of[g, mine, me.c, f] = normed(f)
        copies = [row_copy(g, mine, me.c, 0, me.other_z())]
        copies += [row_copy(g, mine, me.c, s, me.at_x(s)) for s in range(1, nx)]
        copies += [row_copy(g, mine, me.c, nx, me.other_core())]
        for copy in copies:
            copy.start()
        row_sends.extend(copies)

    def get_rows(g):
        slot = nx + 1
        moves = [(rest, True)]
        moves += [(me.zp * nx + (me.x + s) % nx, False) for s in range(1, nx)]
        moves += [((1 - me.zp) * nx + (me.x + s) % nx, False) for s in range(1, nx)]
        for p, across in moves:
            row_wait(g, p, me.c)
            copies = []
            if across:
                for s in range(1, nx):
                    copies.append(row_copy(g, p, me.c, slot, me.at_x(s)))
                    slot += 1
            copies.append(row_copy(g, p, me.c, slot, me.other_core()))
            slot += 1
            for copy in copies:
                copy.start()
            row_sends.extend(copies)
        for p in range(chips):
            row_wait(g, p, 1 - me.c)

    def core_part(g, f):
        return remote(xs.at[f], xr.at[f], xss.at[g, f], xsr.at[g, f], me.other_core())

    def x_part(g, f, s):
        return remote(
            ys.at[f, s - 1], yr.at[f, s - 1], yss.at[g, f, s - 1], ysr.at[g, f, s - 1], me.at_x(s)
        )

    def z_part(g, f):
        return remote(zs.at[f], zr.at[f], zss.at[g, f], zsr.at[g, f], me.other_z())

    def reduce_rows(g, s, hidden):
        last = MATS - 1

        def use(f):
            weight = weights[s][last, f]
            term = jnp.dot(hidden[1 - me.c], weight, preferred_element_type=jnp.float32)
            xs[f] = term.astype(jnp.bfloat16).reshape(chips, r, dn)
            core_part(g, f).start()
            term = jnp.dot(hidden[me.c], weight, preferred_element_type=jnp.float32)
            core_part(g, f).wait_recv()
            part[...] = term.reshape(chips, r, dn) + xr[f].astype(jnp.float32)
            for d in range(1, nx):
                for h in range(PAIR):
                    ys[f, d - 1, h] = part[h * nx + (me.x + d) % nx].astype(jnp.bfloat16)
                x_part(g, f, d).start()
            for h in range(PAIR):
                own[f, h] = part[h * nx + me.x]

        def pass_on(f):
            total = own[f, 1 - me.zp]
            for d in range(1, nx):
                x_part(g, f, d).wait_recv()
                total = total + yr[f, d - 1, 1 - me.zp].astype(jnp.float32)
            zs[f] = total.astype(jnp.bfloat16)
            z_part(g, f).start()

        def step(i, carry):
            @pl.when(i < nz)
            def _():
                @pl.when(i > 0)
                def _():
                    f = me.f_at(i, 0)
                    arrived(s, last, f)
                    for j in range(1, ny):
                        remote(
                            weights[s].at[last, f],
                            weights[s].at[last, f],
                            ysend.at[s, last, i, j],
                            rw.at[s, last, f],
                            me.at_y(j),
                        ).start()

                @pl.when(i == 0)
                def _():
                    local_piece(s, last).wait()

                use(me.f_at(i, 0))

            @pl.when((i >= 1) & (i <= nz))
            def _():
                for j in range(1, ny):
                    f = me.f_at(i - 1, j)
                    arrived(s, last, f)
                    use(f)
                pass_on(me.f_at(i - 1, 0))

            @pl.when(i >= 2)
            def _():
                for j in range(1, ny):
                    pass_on(me.f_at(i - 2, j))

            return carry

        lax.fori_loop(0, nz + 2, step, 0)

    def drain(g):
        def one(f, carry):
            core_part(g, f).wait_send()
            for d in range(1, nx):
                x_part(g, f, d).wait_send()
            z_part(g, f).wait_send()
            return carry

        lax.fori_loop(0, n, one, 0)

    def reduced(g, f):
        z_part(g, f).wait_recv()
        total = own[f, me.zp]
        for d in range(1, nx):
            total = total + yr[f, d - 1, me.zp].astype(jnp.float32)
        return total + zr[f].astype(jnp.float32)

    def hidden_rows(g, s):
        def side(c, carry):
            acc[...] = jnp.zeros_like(acc)

            def feature(f, carry):
                rows = rows_of[g, :, c, f].reshape(chips * r, dn)
                for k in range(MATS - 1):
                    acc[k] += dot_nt(rows, weights[s][k, f])
                return carry

            lax.fori_loop(0, n, feature, 0)
            gate = acc[0]
            hid[c] = (gate * sigmoid(gate) * acc[1]).astype(jnp.bfloat16)
            return carry

        lax.fori_loop(0, CORES, side, 0)

    def mix_rows(g, s):
        acc_m[...] = jnp.zeros_like(acc_m)
        length = nx * CORES * r

        def feature(f, carry):
            rows = rows_of[g, :, :, f].reshape(PAIR * length, dn)
            for k in range(MATS - 1):
                acc_m[k] += dot_nt(rows, weights[s][k, f])
            return carry

        lax.fori_loop(0, n, feature, 0)
        tap = taps[me.zp].astype(jnp.float32)
        a, b = gate_a[me.zp], gate_x[me.zp]
        fall = slope[me.zp]
        for q in range(PAIR):
            rows = pl.ds(q * length, length)
            lru = acc_m[0, rows].astype(jnp.bfloat16).astype(jnp.float32)
            gated = acc_m[1, rows].astype(jnp.bfloat16).astype(jnp.float32)
            conv = tap[0:1] * lru
            for k in range(1, tap.shape[0]):
                conv = conv + tap[k : k + 1] * shift_down(lru, k, 0.0)
            low = conv.astype(jnp.bfloat16)
            recall = sigmoid(jnp.dot(low, a, preferred_element_type=jnp.float32))
            admit = sigmoid(jnp.dot(low, b, preferred_element_type=jnp.float32))
            log_keep = -8.0 * recall * fall
            keep = jnp.exp(log_keep)
            grow = -jnp.tanh(log_keep) * (1.0 + keep * keep)
            state = jnp.sqrt(grow) * admit * low.astype(jnp.float32)
            step = 1
            while step < length:
                state = state + keep * shift_down(state, step, 0.0)
                keep = keep * shift_down(keep, step, 1.0)
                step *= 2
            inner = 0.7978845608028654 * (gated + 0.044715 * gated * gated * gated)
            mixed = state * (0.5 * gated * (1.0 + jnp.tanh(inner)))
            mixed = mixed.astype(jnp.bfloat16)
            for x in range(nx):
                for c in range(CORES):
                    at = (x * CORES + c) * r
                    hid_m[c, pl.ds((q * nx + x) * r, r)] = mixed[at : at + r]

    send_rows(0, lambda f: tokens[f].astype(jnp.float32), gain1)
    for s in range(2):
        for k in range(MATS):
            send_weights(s, k)
    get_rows(0)
    for k in range(MATS - 1):
        for i in range(1, nz):
            forward(0, k, i)
    for k in range(MATS - 1):
        collect(0, k)
    hidden_rows(0, 0)
    reduce_rows(0, 0, hid)
    send_weights(2, 0)
    for f in range(n):
        res[f] = (tokens[f].astype(jnp.float32) + 0.5 * reduced(0, f)).astype(jnp.bfloat16)
    send_rows(1, lambda f: res[f].astype(jnp.float32), gainm)
    send_weights(2, 1)
    for k in range(MATS - 1):
        for i in range(1, nz):
            forward(1, k, i)
    get_rows(1)
    for k in range(MATS - 1):
        collect(1, k)
    mix_rows(1, 1)
    drain(0)
    reduce_rows(1, 1, hid_m)
    send_weights(2, 2)
    for i in range(1, nz):
        forward(2, 0, i)
    for f in range(n):
        res[f] = (res[f].astype(jnp.float32) + reduced(1, f)).astype(jnp.bfloat16)
    send_rows(2, lambda f: res[f].astype(jnp.float32), gain2)
    get_rows(2)
    for i in range(1, nz):
        forward(2, 1, i)
    for k in range(MATS - 1):
        collect(2, k)
    hidden_rows(2, 2)
    drain(1)
    reduce_rows(2, 2, hid)
    for f in range(n):
        out[f] = (res[f].astype(jnp.float32) + 0.5 * reduced(2, f)).astype(jnp.bfloat16)

    for copy in row_sends:
        copy.wait_send()
    for s in range(3):
        for k in range(MATS):
            for i in range(1, nz):
                z_piece(s, k, i).wait_send()
            for i in range(nz):
                for j in range(1, ny):
                    y_piece(s, k, i, j).wait_send()

    drain(2)


def body(
    n,
    t,
    tokens,
    ffn1_gain,
    ffn1_gate,
    ffn1_up,
    ffn1_down,
    mix_gain,
    lru_in_weight,
    lru_gate_weight,
    conv_weight,
    gate_a_weight,
    gate_x_weight,
    decay_param,
    mix_out_weight,
    ffn2_gain,
    ffn2_gate,
    ffn2_up,
    ffn2_down,
):
    r, width = tokens.shape
    dn = width // n
    ny = math.isqrt(n // PAIR)
    nz, nx = n // ny, t // CORES
    chips = PAIR * nx
    hs = ffn1_gate.shape[1] // PAIR
    size = gate_a_weight.shape[1]
    extra = -gate_a_weight.shape[0] % PAIR
    if extra:
        lru_in_weight, lru_gate_weight, conv_weight = (
            jnp.pad(w, ((0, 0), (0, extra * size))) for w in (lru_in_weight, lru_gate_weight, conv_weight)
        )
        gate_a_weight, gate_x_weight = (
            jnp.pad(w, ((0, extra), (0, 0), (0, 0))) for w in (gate_a_weight, gate_x_weight)
        )
        decay_param = jnp.pad(decay_param, (0, extra * size))
        mix_out_weight = jnp.pad(mix_out_weight, ((0, extra * size), (0, 0)))
    cs = lru_in_weight.shape[1] // PAIR
    count = gate_a_weight.shape[0] // PAIR

    def halves(first, second, third):
        return [w.reshape(PAIR, -1, dn) for w in (first.T, second.T, third)]

    def blocks(v):
        return v.reshape(n, 1, dn)

    eye = jnp.eye(count, dtype=jnp.bfloat16)

    def dense(weight):
        weight = weight.reshape(PAIR, count, size, size)
        return (eye[:, None, :, None] * weight[:, :, :, None, :]).reshape(PAIR, cs, cs)

    small = [
        tokens.reshape(r, n, dn).transpose(1, 0, 2),
        blocks(ffn1_gain),
        blocks(mix_gain),
        blocks(ffn2_gain),
        conv_weight.reshape(-1, PAIR, cs).transpose(1, 0, 2),
        dense(gate_a_weight),
        dense(gate_x_weight),
        jax.nn.softplus(-decay_param).reshape(PAIR, 1, cs),
    ]
    big = (
        halves(ffn1_gate, ffn1_up, ffn1_down)
        + halves(lru_in_weight, lru_gate_weight, mix_out_weight)
        + halves(ffn2_gate, ffn2_up, ffn2_down)
    )
    bf16, f32 = jnp.bfloat16, jnp.float32
    sem = pltpu.SemaphoreType.DMA
    scratch = [
        pltpu.VMEM((MATS, n, hs, dn), bf16),
        pltpu.VMEM((MATS, n, cs, dn), bf16),
        pltpu.VMEM((MATS, n, hs, dn), bf16),
        pltpu.VMEM((3, chips, CORES, n, r, dn), bf16),
        pltpu.VMEM((n, chips, r, dn), bf16),
        pltpu.VMEM((n, chips, r, dn), bf16),
        pltpu.VMEM((n, nx - 1, PAIR, r, dn), bf16),
        pltpu.VMEM((n, nx - 1, PAIR, r, dn), bf16),
        pltpu.VMEM((n, r, dn), bf16),
        pltpu.VMEM((n, r, dn), bf16),
        pltpu.VMEM((n, PAIR, r, dn), f32),
        pltpu.VMEM((chips, r, dn), f32),
        pltpu.VMEM((CORES, chips * r, hs), bf16),
        pltpu.VMEM((MATS - 1, chips * r, hs), f32),
        pltpu.VMEM((CORES, chips * r, cs), bf16),
        pltpu.VMEM((MATS - 1, CORES * chips * r, cs), f32),
        pltpu.VMEM((n, r, dn), bf16),
        sem((3, MATS, n)),
        sem((3, MATS, nz)),
        sem((3, MATS, nz, ny)),
        sem((3, MATS)),
        sem((3, chips, CORES)),
        sem((3, 4 * nx)),
        sem((3, n)),
        sem((3, n)),
        sem((3, n, nx - 1)),
        sem((3, n, nx - 1)),
        sem((3, n)),
        sem((3, n)),
    ]
    vmem = pl.BlockSpec(memory_space=pltpu.VMEM)
    hbm = pl.BlockSpec(memory_space=pl.ANY)
    result = pl.pallas_call(
        functools.partial(layer_kernel, n, t),
        out_shape=jax.ShapeDtypeStruct((n, r, dn), bf16),
        in_specs=[vmem] * len(small) + [hbm] * len(big),
        out_specs=vmem,
        scratch_shapes=scratch,
        compiler_params=pltpu.CompilerParams(
            collective_id=0, has_side_effects=True, vmem_limit_bytes=66_000_000
        ),
    )(*small, *big)
    return result.transpose(1, 0, 2).reshape(r, width)


def solution(mesh):
    n, t = mesh.shape["fs"], mesh.shape["tp"]
    in_specs = (
        P(("fs", "tp"), None),
        P(),
        P("fs", "tp"),
        P("fs", "tp"),
        P("tp", "fs"),
        P(),
        P("fs", "tp"),
        P("fs", "tp"),
        P(None, "tp"),
        P("tp", None, None),
        P("tp", None, None),
        P("tp"),
        P("tp", "fs"),
        P(),
        P("fs", "tp"),
        P("fs", "tp"),
        P("tp", "fs"),
    )

    def run(*args):
        return body(n, t, *args)

    return jax.shard_map(
        run, mesh=mesh, in_specs=in_specs, out_specs=P(("fs", "tp"), None), check_vma=False
    )
```

profile of v0, /device:TPU:0, one launch (start us, length us, event | category | flops | bytes accessed | tf_op | source)
XLA Modules:
  0.0 356.5 jit_solution(11454157112892966025)
XLA Ops:
  0.0 0.0 copy-start.10
  0.0 0.7 copy-done.10
  0.7 0.0 copy-start.9
  0.7 0.7 reshape.69.refs_7_
  1.4 0.0 copy-done.9
  1.4 0.1 reshape.68
  1.5 0.6 copy.38
  2.1 0.1 mul.44
  2.2 0.0 copy-start.5
  2.2 0.0 copy-start.6
  2.2 0.2 mul.45
  2.4 0.7 copy-done.5
  3.1 0.0 copy-start.4
  3.1 0.8 copy.28
  3.9 0.0 copy-done.6
  3.9 0.8 copy.29
  4.8 0.0 copy-done.4
  4.8 0.0 copy-start.7
  4.8 0.8 copy.37
  5.5 0.1 copy-done.7
  5.7 0.1 mul.48
  5.8 0.0 copy-start.8
  5.8 0.2 mul.49
  6.0 0.6 copy-done.8
  6.7 0.1 mul.52
  6.8 0.0 copy-start
  6.8 0.2 mul.53
  7.0 0.8 broadcast_multiply_fusion
  7.8 0.0 copy-done
  7.9 0.0 copy-start.1
  7.9 1.1 copy.26
  9.0 0.0 copy-done.1
  9.0 0.0 copy-start.2
  9.0 1.1 copy.27
  10.2 0.0 copy-done.2
  10.2 0.0 copy-start.3
  10.2 1.2 copy.30
  11.3 0.0 copy-done.3
  11.3 1.1 copy.31
  12.5 342.3 %shard_map.163 = bf16[8,96,256]{2,1,0:T(8,128)(2,1)} custom-call(bf16[8,96,256]{2,1,0:T(8,128)(2,1)} %bitcast.37, f32[8,1,256]{2,1,0:T(1,128)} %bitcast.54, f32[8,1,256]{2,1,0:T(1,128)} %bitcast.55, f32[8,1,256]{2,1,0:T(1,128)} %bitcast.56, bf16[2,4,192]{2,1,0:T(4,128)(2,1)} %bitcast.53, bf16[2,192,192]{2,1,0:T(8,128)(2,1)} %get-tuple-element.6.refs_5_, ...), custom_call_target="tpu_custom_call" | custom-call | tf_op jit(solution)/shard_map/pallas_call | solution.py:503
  354.7 1.8 copy.34
  (2 shorter events, 0.0 us)
Async XLA Ops:
  0.0 0.7 copy-start.10
  0.7 0.7 copy-start.9
  2.2 0.9 copy-start.5
  2.2 1.7 copy-start.6
  3.1 1.6 copy-start.4
  4.8 0.9 copy-start.7
  5.8 0.9 copy-start.8
  6.8 1.1 copy-start
  7.9 1.1 copy-start.1
  9.0 1.2 copy-start.2
  10.2 1.2 copy-start.3
where the time goes:
time: 357 us
  Pallas kernels  342 us (96%)
  local copies, waits for them, and re-layouts  13.4 us (4%)
    pallas_call x1, Pallas kernels, body(): pl.pallas_call(functools.partial(layer_kernel, n, t), out_shape=jax.Shape...  342 us

commit v1 on v0

v1 whole, which is shorter than its diff:
```python
import functools
import math

import jax
import jax.numpy as jnp
from jax import lax
from jax.experimental import pallas as pl
from jax.experimental.pallas import tpu as pltpu
from jax.sharding import PartitionSpec as P

EPS = 1e-06
CORES = 2
PAIR = 2
MATS = 3
ROW_PARTS = 4
MESH = pl.DeviceIdType.MESH


def dot_nt(a, b):
    return lax.dot_general(a, b, (((1,), (1,)), ((), ())), preferred_element_type=jnp.float32)


def sigmoid(v):
    return 1.0 / (1.0 + jnp.exp(-v))


def shift_down(values, step, fill):
    pad = jnp.full((step, values.shape[1]), fill, values.dtype)
    return jnp.concatenate([pad, values[: values.shape[0] - step]], axis=0)


class Place:
    def __init__(self, n, t):
        self.n, self.t = n, t
        self.ny = math.isqrt(n // PAIR)
        self.nz = n // self.ny
        self.nq = self.nz // PAIR
        self.nx = t // CORES
        fs, tp = lax.axis_index("fs"), lax.axis_index("tp")
        self.fs, self.tp = fs, tp
        self.z, self.y = fs // self.ny, fs % self.ny
        self.q, self.zp = self.z // PAIR, self.z % PAIR
        self.x, self.c = tp // CORES, tp % CORES
        self.chips = PAIR * self.nx
        self.inner = (self.q + self.zp) % PAIR

    def z_at(self, i):
        q = (self.q + i // PAIR) % self.nq
        turn = self.inner * (1 if i >= PAIR else 0) if isinstance(i, int) else jnp.where(i >= PAIR, self.inner, 0)
        return q * PAIR + (self.zp + i + turn) % PAIR

    def f_at(self, i, j):
        return self.z_at(i) * self.ny + (self.y + j) % self.ny

    def at_z(self, z):
        return (z * self.ny + self.y, self.tp)

    def at_y(self, j):
        return (self.z * self.ny + (self.y + j) % self.ny, self.tp)

    def at_x(self, s):
        return (self.fs, ((self.x + s) % self.nx) * CORES + self.c)

    def other_z(self):
        return self.at_z(self.q * PAIR + 1 - self.zp)

    def other_core(self):
        return (self.fs, self.x * CORES + 1 - self.c)


def remote(src, dst, send, recv, device):
    return pltpu.make_async_remote_copy(
        src_ref=src, dst_ref=dst, send_sem=send, recv_sem=recv, device_id=device, device_id_type=MESH
    )


def layer_kernel(n, t, *refs):
    (tokens_in, gain1, gainm, gain2, taps, gate_a, gate_x, slope) = refs[:8]
    raw = (refs[8:11], refs[11:14], refs[14:17])
    out = refs[17]
    (w1, wm, w2, rel1, relm, rel2, rows_of, xs, xr, ys, yr, zs, zr, own, part_sum, hid, acc, hid_m, acc_m, res, tokens, load1, loadm, load2, flip1, flipm, flip2, wide_a, wide_x) = refs[18:47]
    (rw, rrel, zsend, ysend, lsem, gr, gs, xss, xsr, yss, ysr, zss, zsr, load_sem) = refs[47:]
    weights = (w1, wm, w2)
    relays = (rel1, relm, rel2)
    me = Place(n, t)
    r, width = tokens_in.shape
    dn = width // n
    loads, flips = (load1, loadm, load2), (flip1, flipm, flip2)
    sources = [
        [flips[s].at[k] for k in range(MATS - 1)]
        + [raw[s][MATS - 1]]
        for s in range(3)
    ]

    def load(s, k):
        return pltpu.make_async_copy(raw[s][k], loads[s].at[k], load_sem.at[s, k])

    def flip(s, k):
        load(s, k).wait()
        flips[s][k] = loads[s][k].T.reshape(flips[s].shape[1:])

    for s in range(3):
        for k in range(MATS - 1):
            load(s, k).start()
    chips, nx, ny, nz = me.chips, me.nx, me.ny, me.nz
    parts = math.gcd(n, ROW_PARTS)
    step = n // parts
    mine = me.zp * nx + me.x
    rest = (1 - me.zp) * nx + me.x

    barrier = pltpu.get_barrier_semaphore()
    peers = [me.at_z((me.z + d) % nz) for d in range(1, nz)]
    peers += [me.at_y(j) for j in range(1, ny)]
    peers += [me.at_x(s) for s in range(1, nx)]
    peers += [me.other_core()]
    for peer in peers:
        pl.semaphore_signal(barrier, inc=1, device_id=peer, device_id_type=MESH)
    flip(0, 0)
    for f in range(n):
        tokens[f] = tokens_in[:, f * dn : (f + 1) * dn]
    pl.semaphore_wait(barrier, len(peers))

    def z_piece(s, k, i):
        z = me.z_at(i)
        return remote(
            sources[s][k].at[z % PAIR],
            weights[s].at[k, me.fs],
            zsend.at[s, k, i],
            rw.at[s, k, me.fs],
            me.at_z(z),
        )

    def y_piece(s, k, i, j):
        f = me.f_at(i, 0)
        src = sources[s][k].at[me.zp] if isinstance(i, int) and i == 0 else weights[s].at[k, f]
        return remote(
            src, weights[s].at[k, f], ysend.at[s, k, i, j], rw.at[s, k, f], me.at_y(j)
        )

    def local_piece(s, k):
        return pltpu.make_async_copy(
            sources[s][k].at[me.zp], weights[s].at[k, me.fs], lsem.at[s, k]
        )

    def arrived(s, k, f):
        place = weights[s].at[k, f]
        remote(place, place, zsend.at[s, k, 0], rw.at[s, k, f], me.at_y(0)).wait_recv()

    def relay_in(s, k):
        return remote(
            sources[s][k].at[me.zp],
            relays[s].at[k],
            zsend.at[s, k, 0],
            rrel.at[s, k],
            me.other_z(),
        )

    def relay_near(s, k, i):
        f = me.f_at(1, 0)
        place = weights[s].at[k, f]
        return remote(place, place, zsend.at[s, k, nz + i], rw.at[s, k, f], me.at_z(me.z_at(i)))

    def relay_out(s, k, i):
        f = me.f_at(1, 0)
        return remote(
            relays[s].at[k],
            weights[s].at[k, f],
            zsend.at[s, k, nz + i],
            rw.at[s, k, f],
            me.at_z(me.z_at(i)),
        )

    def when_inner(*actions):
        @pl.when(me.inner == 1)
        def _():
            for act, s, k in actions:
                act(s, k)

    def when_end(*actions):
        @pl.when(me.inner == 0)
        def _():
            for act, s, k in actions:
                act(s, k)

    def send_cross(s, k):
        for i in range(PAIR, nz):
            z_piece(s, k, i).start()

    def send_near(s, k):
        z_piece(s, k, 1).start()

    def send_both(s, k):
        send_near(s, k)
        relay_in(s, k).start()

    def relay(s, k):
        relay_in(s, k).wait_recv()
        for i in range(PAIR, nz, 2):
            relay_out(s, k, i).start()

    def send_own(s, k):
        for j in range(1, ny):
            y_piece(s, k, 0, j).start()
        local_piece(s, k).start()

    def forward(s, k, i):
        arrived(s, k, me.f_at(i, 0))
        for j in range(1, ny):
            y_piece(s, k, i, j).start()
        if i == 1:

            @pl.when(me.inner == 1)
            def _():
                for m in range(PAIR + 1, nz, 2):
                    relay_near(s, k, m).start()

    def collect(s, k):
        local_piece(s, k).wait()
        for i in range(nz):
            for j in range(1, ny):
                arrived(s, k, me.f_at(i, j))

    def row_copy(g, p, c, slot, part, device):
        block = rows_of.at[g, p, c, pl.ds(part * step, step)]
        return remote(block, block, gs.at[g, slot, part], gr.at[g, p, c, part], device)

    def row_wait(g, p, c, part):
        row_copy(g, p, c, 0, part, me.other_core()).wait_recv()

    def norm_rows(values, gain):
        total = jnp.zeros((r, 1), jnp.float32)
        for f in range(n):
            wide = values(f)
            total += jnp.sum(wide * wide, axis=-1, keepdims=True)
        scale = lax.rsqrt(total / width + EPS)
        return lambda f: (values(f) * scale * gain[:, f * dn : (f + 1) * dn]).astype(jnp.bfloat16)

    row_sends = []

    def send_rows(g, values, gain):
        normed = norm_rows(values, gain)
        for f in range(n):
            rows_of[g, mine, me.c, f] = normed(f)
        targets = [me.other_z()] + [me.at_x(d) for d in range(1, nx)] + [me.other_core()]
        for slot, device in enumerate(targets):
            for part in range(parts):
                copy = row_copy(g, mine, me.c, slot, part, device)
                copy.start()
                row_sends.append(copy)

    def spread(g, p, slot, part, across):
        row_wait(g, p, me.c, part)
        targets = [me.at_x(d) for d in range(1, nx)] if across else []
        targets += [me.other_core()]
        for m, device in enumerate(targets):
            copy = row_copy(g, p, me.c, slot + m, part, device)
            copy.start()
            row_sends.append(copy)

    def near_rows(g):
        for part in range(parts):
            spread(g, rest, nx + 1, part, True)

    def far_rows(g):
        slot = 2 * nx + 1
        for base in (me.zp * nx, (1 - me.zp) * nx):
            for d in range(1, nx):
                for part in range(parts):
                    spread(g, base + (me.x + d) % nx, slot, part, False)
                slot += 1
        for p in range(chips):
            for part in range(parts):
                row_wait(g, p, 1 - me.c, part)

    def core_part(g, f):
        return remote(xs.at[f], xr.at[f], xss.at[g, f], xsr.at[g, f], me.other_core())

    def x_part(g, f, s):
        return remote(
            ys.at[f, s - 1], yr.at[f, s - 1], yss.at[g, f, s - 1], ysr.at[g, f, s - 1], me.at_x(s)
        )

    def z_part(g, f):
        return remote(zs.at[f], zr.at[f], zss.at[g, f], zsr.at[g, f], me.other_z())

    order = [(0, 0)]
    for i in range(1, nz + 1):
        order += [(i, 0)] if i < nz else []
        order += [(i - 1, j) for j in range(1, ny)]

    def reduce_rows(g, s, hidden, early=(), paced=False):
        last = MATS - 1

        def begin(m):
            i, j = order[m]
            f = me.f_at(i, j)
            if j:
                arrived(s, last, f)
            elif i == 0:
                local_piece(s, last).wait()
            elif i not in early:
                forward(s, last, i)
            weight = weights[s][last, f]
            term = jnp.dot(hidden[1 - me.c], weight, preferred_element_type=jnp.float32)
            xs[f] = term.astype(jnp.bfloat16).reshape(chips, r, dn)
            core_part(g, f).start()
            term = jnp.dot(hidden[me.c], weight, preferred_element_type=jnp.float32)
            part_sum[m % 2] = term.reshape(chips, r, dn)

        def cross(m):
            f = me.f_at(*order[m])
            core_part(g, f).wait_recv()
            for h in range(PAIR):
                for d in range(1, nx):
                    p = h * nx + (me.x + d) % nx
                    total = part_sum[m % 2, p] + xr[f, p].astype(jnp.float32)
                    ys[f, d - 1, h] = total.astype(jnp.bfloat16)
            for d in range(1, nx):
                x_part(g, f, d).start()
            for h in range(PAIR):
                p = h * nx + me.x
                own[f, h] = part_sum[m % 2, p] + xr[f, p].astype(jnp.float32)

        def pass_on(m):
            f = me.f_at(*order[m])
            total = own[f, 1 - me.zp]
            for d in range(1, nx):
                x_part(g, f, d).wait_recv()
                total = total + yr[f, d - 1, 1 - me.zp].astype(jnp.float32)
            zs[f] = total.astype(jnp.bfloat16)
            z_part(g, f).start()

        for m in range(n + 3):
            if paced and 1 <= m <= n:
                cross(m - 1)
            if m < n:
                begin(m)
            if not paced and 1 <= m <= n:
                cross(m - 1)
            if m >= 3:
                pass_on(m - 3)

    def reduced(g, f):
        z_part(g, f).wait_recv()
        total = own[f, me.zp]
        for d in range(1, nx):
            total = total + yr[f, d - 1, me.zp].astype(jnp.float32)
        return total + zr[f].astype(jnp.float32)

    def drain(g):
        def one(f, carry):
            core_part(g, f).wait_send()
            for d in range(1, nx):
                x_part(g, f, d).wait_send()
            z_part(g, f).wait_send()
            return carry

        lax.fori_loop(0, n, one, 0)

    def project(g, s, k, c, to):
        acc[to] = jnp.zeros_like(acc[to])

        def feature(f, carry):
            rows = rows_of[g, :, c, f].reshape(chips * r, dn)
            acc[to] += dot_nt(rows, weights[s][k, f])
            return carry

        lax.fori_loop(0, n, feature, 0)

    def gate_rows(g, s):
        def side(c, carry):
            project(g, s, 0, c, c)
            return carry

        lax.fori_loop(0, CORES, side, 0)

    def hidden_rows(g, s):
        def side(c, carry):
            project(g, s, 1, c, CORES)
            gate = acc[c]
            hid[c] = (gate * sigmoid(gate) * acc[CORES]).astype(jnp.bfloat16)
            return carry

        lax.fori_loop(0, CORES, side, 0)

    def mix_rows(g, s):
        acc_m[...] = jnp.zeros_like(acc_m)
        length = nx * CORES * r

        def feature(f, carry):
            rows = rows_of[g, :, :, f].reshape(PAIR * length, dn)
            for k in range(MATS - 1):
                acc_m[k] += dot_nt(rows, weights[s][k, f])
            return carry

        lax.fori_loop(0, n, feature, 0)
        channels = taps.shape[1] // PAIR

        def mine_of(v):
            return jnp.where(me.zp == 0, v[:, :channels], v[:, channels:])

        tap = mine_of(taps[...].astype(jnp.float32))
        fall = mine_of(slope[...])
        count, size = gate_a.shape[0] // PAIR, gate_a.shape[1]
        for wide, gate in ((wide_a, gate_a), (wide_x, gate_x)):
            wide[...] = jnp.zeros_like(wide)
            for m in range(count):
                at = slice(m * size, (m + 1) * size)
                wide[at, at] = gate[me.zp * count + m].astype(jnp.float32)
        a, b = wide_a[...].astype(jnp.bfloat16), wide_x[...].astype(jnp.bfloat16)
        for q in range(PAIR):
            rows = pl.ds(q * length, length)
            lru = acc_m[0, rows].astype(jnp.bfloat16).astype(jnp.float32)
            gated = acc_m[1, rows].astype(jnp.bfloat16).astype(jnp.float32)
            conv = tap[0:1] * lru
            for k in range(1, tap.shape[0]):
                conv = conv + tap[k : k + 1] * shift_down(lru, k, 0.0)
            low = conv.astype(jnp.bfloat16)
            recall = sigmoid(jnp.dot(low, a, preferred_element_type=jnp.float32))
            admit = sigmoid(jnp.dot(low, b, preferred_element_type=jnp.float32))
            log_keep = -8.0 * recall * fall
            keep = jnp.exp(log_keep)
            grow = -jnp.tanh(log_keep) * (1.0 + keep * keep)
            state = jnp.sqrt(grow) * admit * low.astype(jnp.float32)
            step = 1
            while step < length:
                state = state + keep * shift_down(state, step, 0.0)
                keep = keep * shift_down(keep, step, 1.0)
                step *= 2
            inner = 0.7978845608028654 * (gated + 0.044715 * gated * gated * gated)
            mixed = state * (0.5 * gated * (1.0 + jnp.tanh(inner)))
            mixed = mixed.astype(jnp.bfloat16)
            for x in range(nx):
                for c in range(CORES):
                    at = (x * CORES + c) * r
                    hid_m[c, pl.ds((q * nx + x) * r, r)] = mixed[at : at + r]

    first = range(PAIR, nz, PAIR)
    second = range(PAIR + 1, nz, PAIR)

    def forward_all(s, k, which):
        for i in which:
            forward(s, k, i)

    when_end((send_both, 0, 0))
    when_inner((send_near, 0, 0), (send_cross, 0, 0))
    send_own(0, 0)
    send_rows(0, lambda f: tokens[f].astype(jnp.float32), gain1)
    flip(0, 1)
    when_end((send_both, 0, 1), (send_both, 0, 2))
    when_inner((send_near, 0, 1), (send_near, 0, 2), (send_cross, 0, 1))
    send_own(0, 1)
    send_own(0, 2)
    for s in (1, 2):
        for k in range(MATS - 1):
            flip(s, k)
    for k in range(MATS):
        send_own(1, k)
    send_own(2, 0)
    forward_all(0, 0, [1])
    when_inner((relay, 0, 0), (send_cross, 0, 2))
    near_rows(0)
    forward_all(0, 0, first)
    far_rows(0)
    forward_all(0, 0, second)
    forward_all(0, 1, [1])
    when_inner((relay, 0, 1), (send_near, 2, 0))
    collect(0, 0)
    when_end(*[(send_both, 1, k) for k in range(MATS)], (send_both, 2, 0), (send_both, 2, 1))
    gate_rows(0, 0)
    forward_all(0, 1, first)
    forward_all(0, 2, [1])
    when_inner((relay, 0, 2))
    forward_all(0, 1, second)
    when_inner(*[(act, 1, k) for k in range(MATS) for act in (send_near, send_cross, relay)])
    collect(0, 1)
    for k in range(MATS):
        forward_all(1, k, [1])
    when_inner((send_near, 2, 1))
    hidden_rows(0, 0)
    reduce_rows(0, 0, hid, [1], True)
    when_inner((send_cross, 2, 0), (send_cross, 2, 1), (send_cross, 2, 2))
    for f in range(n):
        res[f] = (tokens[f].astype(jnp.float32) + 0.5 * reduced(0, f)).astype(jnp.bfloat16)
    send_rows(1, lambda f: res[f].astype(jnp.float32), gainm)
    when_end((send_both, 2, 2))
    for k in range(MATS):
        forward_all(1, k, range(2, nz))
    forward_all(2, 0, [1])
    when_inner((relay, 2, 0), (relay, 2, 1))
    near_rows(1)
    when_inner((send_near, 2, 2))
    send_own(2, 1)
    far_rows(1)
    for k in range(MATS - 1):
        collect(1, k)
    forward_all(2, 1, [1])
    mix_rows(1, 1)
    forward_all(2, 0, first)
    send_own(2, 2)
    drain(0)
    reduce_rows(1, 1, hid_m, range(1, nz))
    forward_all(2, 2, [1])
    when_inner((relay, 2, 2))
    forward_all(2, 1, first)
    for f in range(n):
        res[f] = (res[f].astype(jnp.float32) + reduced(1, f)).astype(jnp.bfloat16)
    send_rows(2, lambda f: res[f].astype(jnp.float32), gain2)
    forward_all(2, 2, first)
    forward_all(2, 0, second)
    near_rows(2)
    far_rows(2)
    forward_all(2, 1, second)
    collect(2, 0)
    gate_rows(2, 2)
    collect(2, 1)
    hidden_rows(2, 2)
    drain(1)
    reduce_rows(2, 2, hid, [1, *first], True)
    for f in range(n):
        out[f] = (res[f].astype(jnp.float32) + 0.5 * reduced(2, f)).astype(jnp.bfloat16)

    for copy in row_sends:
        copy.wait_send()
    for s in range(3):
        for k in range(MATS):
            z_piece(s, k, 1).wait_send()
            for i in range(nz):
                for j in range(1, ny):
                    y_piece(s, k, i, j).wait_send()

    def finish_inner(s, k):
        for i in range(PAIR, nz):
            z_piece(s, k, i).wait_send()
            (relay_near if i % PAIR else relay_out)(s, k, i).wait_send()

    def finish_end(s, k):
        relay_in(s, k).wait_send()

    when_inner(*[(finish_inner, s, k) for s in range(3) for k in range(MATS)])
    when_end(*[(finish_end, s, k) for s in range(3) for k in range(MATS)])

    drain(2)


def body(
    n,
    t,
    tokens,
    ffn1_gain,
    ffn1_gate,
    ffn1_up,
    ffn1_down,
    mix_gain,
    lru_in_weight,
    lru_gate_weight,
    conv_weight,
    gate_a_weight,
    gate_x_weight,
    decay_param,
    mix_out_weight,
    ffn2_gain,
    ffn2_gate,
    ffn2_up,
    ffn2_down,
):
    r, width = tokens.shape
    dn = width // n
    ny = math.isqrt(n // PAIR)
    nz, nx = n // ny, t // CORES
    chips = PAIR * nx
    parts = math.gcd(n, ROW_PARTS)
    hs = ffn1_gate.shape[1] // PAIR
    size = gate_a_weight.shape[1]
    extra = -gate_a_weight.shape[0] % PAIR
    if extra:
        lru_in_weight, lru_gate_weight, conv_weight = (
            jnp.pad(w, ((0, 0), (0, extra * size))) for w in (lru_in_weight, lru_gate_weight, conv_weight)
        )
        gate_a_weight, gate_x_weight = (
            jnp.pad(w, ((0, extra), (0, 0), (0, 0))) for w in (gate_a_weight, gate_x_weight)
        )
        decay_param = jnp.pad(decay_param, (0, extra * size))
        mix_out_weight = jnp.pad(mix_out_weight, ((0, extra * size), (0, 0)))
    cs = lru_in_weight.shape[1] // PAIR

    small = [
        tokens,
        ffn1_gain[None],
        mix_gain[None],
        ffn2_gain[None],
        conv_weight,
        gate_a_weight,
        gate_x_weight,
        jax.nn.softplus(-decay_param)[None],
    ]
    big = [
        ffn1_gate,
        ffn1_up,
        ffn1_down.reshape(PAIR, hs, dn),
        lru_in_weight,
        lru_gate_weight,
        mix_out_weight.reshape(PAIR, cs, dn),
        ffn2_gate,
        ffn2_up,
        ffn2_down.reshape(PAIR, hs, dn),
    ]
    bf16, f32 = jnp.bfloat16, jnp.float32
    sem = pltpu.SemaphoreType.DMA
    scratch = [
        pltpu.VMEM((MATS, n, hs, dn), bf16),
        pltpu.VMEM((MATS, n, cs, dn), bf16),
        pltpu.VMEM((MATS, n, hs, dn), bf16),
        pltpu.VMEM((MATS, hs, dn), bf16),
        pltpu.VMEM((MATS, cs, dn), bf16),
        pltpu.VMEM((MATS, hs, dn), bf16),
        pltpu.VMEM((3, chips, CORES, n, r, dn), bf16),
        pltpu.VMEM((n, chips, r, dn), bf16),
        pltpu.VMEM((n, chips, r, dn), bf16),
        pltpu.VMEM((n, nx - 1, PAIR, r, dn), bf16),
        pltpu.VMEM((n, nx - 1, PAIR, r, dn), bf16),
        pltpu.VMEM((n, r, dn), bf16),
        pltpu.VMEM((n, r, dn), bf16),
        pltpu.VMEM((n, PAIR, r, dn), f32),
        pltpu.VMEM((2, chips, r, dn), f32),
        pltpu.VMEM((CORES, chips * r, hs), bf16),
        pltpu.VMEM((CORES + 1, chips * r, hs), f32),
        pltpu.VMEM((CORES, chips * r, cs), bf16),
        pltpu.VMEM((MATS - 1, CORES * chips * r, cs), f32),
        pltpu.VMEM((n, r, dn), bf16),
        pltpu.VMEM((n, r, dn), bf16),
        *[pltpu.VMEM((MATS - 1, dn, PAIR * u), bf16) for u in (hs, cs, hs)],
        *[pltpu.VMEM((MATS - 1, PAIR, u, dn), bf16) for u in (hs, cs, hs)],
        pltpu.VMEM((cs, cs), f32),
        pltpu.VMEM((cs, cs), f32),
        sem((3, MATS, n)),
        sem((3, MATS)),
        sem((3, MATS, 2 * nz)),
        sem((3, MATS, nz, ny)),
        sem((3, MATS)),
        sem((3, chips, CORES, parts)),
        sem((3, 4 * nx, parts)),
        sem((3, n)),
        sem((3, n)),
        sem((3, n, nx - 1)),
        sem((3, n, nx - 1)),
        sem((3, n)),
        sem((3, n)),
        sem((3, MATS)),
    ]
    vmem = pl.BlockSpec(memory_space=pltpu.VMEM)
    hbm = pl.BlockSpec(memory_space=pl.ANY)
    result = pl.pallas_call(
        functools.partial(layer_kernel, n, t),
        out_shape=jax.ShapeDtypeStruct((n, r, dn), bf16),
        in_specs=[vmem] * len(small) + [hbm] * len(big),
        out_specs=vmem,
        scratch_shapes=scratch,
        compiler_params=pltpu.CompilerParams(
            collective_id=0, has_side_effects=True, vmem_limit_bytes=66_000_000
        ),
    )(*small, *big)
    return result.transpose(1, 0, 2).reshape(r, width)


def solution(mesh):
    n, t = mesh.shape["fs"], mesh.shape["tp"]
    in_specs = (
        P(("fs", "tp"), None),
        P(),
        P("fs", "tp"),
        P("fs", "tp"),
        P("tp", "fs"),
        P(),
        P("fs", "tp"),
        P("fs", "tp"),
        P(None, "tp"),
        P("tp", None, None),
        P("tp", None, None),
        P("tp"),
        P("tp", "fs"),
        P(),
        P("fs", "tp"),
        P("fs", "tp"),
        P("tp", "fs"),
    )

    def run(*args):
        return body(n, t, *args)

    return jax.shard_map(
        run, mesh=mesh, in_specs=in_specs, out_specs=P(("fs", "tp"), None), check_vma=False
    )
```

time: 357 us -> 272 us (0.76)
  Pallas kernels: 342 us -> 268 us
  local copies, waits for them, and re-layouts: 13.4 us -> 3.03 us
    pallas_call x1, Pallas kernels: 342 us -> 268 us  [body(): pl.pallas_call(functools.partial(layer_kernel, n, t), out_shape=jax.Shape...]
    transpose x6 -> x0, local copies, waits for them, and re-layouts: 6.22 us -> none  [halves(): return [w.reshape(PAIR, -1, dn) for w in (first.T, second.T, third)]]
where the time goes in v1:
time: 272 us
  Pallas kernels  268 us (99%)
  local copies, waits for them, and re-layouts  3.03 us (1%)
    pallas_call x1, Pallas kernels, body(): pl.pallas_call(functools.partial(layer_kernel, n, t), out_shape=jax.Shape...  268 us

profile of v1, /device:TPU:0, one launch (start us, length us, event | category | flops | bytes accessed | tf_op | source)
XLA Modules:
  0.0 271.5 jit_solution(11113145190936249118)
XLA Ops:
  0.0 0.0 copy-start
  0.0 0.7 copy-done
  0.7 0.6 broadcast_in_dim.15.refs_7_
  1.3 268.5 %shard_map.163 = bf16[8,96,256]{2,1,0:T(8,128)(2,1)} custom-call(bf16[96,2048]{1,0:T(8,128)(2,1)} %refs_0_.1, f32[1,2048]{1,0:T(1,128)} %bitcast.13, f32[1,2048]{1,0:T(1,128)} %bitcast.14, f32[1,2048]{1,0:T(1,128)} %bitcast.15, bf16[4,384]{1,0:T(4,128)(2,1)} %refs_4_.1, bf16[6,64,64]{2,1,0:T(8,128)(2,1)} %refs_5_.1, bf16[6,64,64]{2,1,0:T(8,128)(2,1)} %refs_6_.1, ...), custom_call_target="tpu_custom_call" | custom-call | tf_op jit(solution)/shard_map/pallas_call | solution.py:653
  269.7 1.8 copy.19
  (1 shorter events, 0.0 us)
Async XLA Ops:
  0.0 0.7 copy-start

commit v2 on v1

--- a/solution.py
+++ b/solution.py
@@ -182,8 +182,12 @@
             for act, s, k in actions:
                 act(s, k)
 
-    def send_cross(s, k):
-        for i in range(PAIR, nz):
+    def to_inner(s, k):
+        for i in range(PAIR, nz, 2):
+            z_piece(s, k, i).start()
+
+    def to_end(s, k):
+        for i in range(PAIR + 1, nz, 2):
             z_piece(s, k, i).start()
 
     def send_near(s, k):
@@ -374,14 +378,13 @@
 
         lax.fori_loop(0, CORES, side, 0)
 
-    def hidden_rows(g, s):
-        def side(c, carry):
+    def hidden_rows(g, s, between=()):
+        for c in (1 - me.c, me.c):
             project(g, s, 1, c, CORES)
             gate = acc[c]
             hid[c] = (gate * sigmoid(gate) * acc[CORES]).astype(jnp.bfloat16)
-            return carry
-
-        lax.fori_loop(0, CORES, side, 0)
+            forward_all(s, MATS - 1, between)
+            between = ()
 
     def mix_rows(g, s):
         acc_m[...] = jnp.zeros_like(acc_m)
@@ -442,79 +445,80 @@
         for i in which:
             forward(s, k, i)
 
+    def take_near(s, k):
+        forward(s, k, 1)
+
     when_end((send_both, 0, 0))
-    when_inner((send_near, 0, 0), (send_cross, 0, 0))
+    when_inner((send_near, 0, 0), (to_inner, 0, 0))
     send_own(0, 0)
     send_rows(0, lambda f: tokens[f].astype(jnp.float32), gain1)
     flip(0, 1)
     when_end((send_both, 0, 1), (send_both, 0, 2))
-    when_inner((send_near, 0, 1), (send_near, 0, 2), (send_cross, 0, 1))
+    when_inner((send_near, 0, 1), (to_inner, 0, 1), (to_end, 0, 0), (send_near, 0, 2))
     send_own(0, 1)
-    send_own(0, 2)
     for s in (1, 2):
         for k in range(MATS - 1):
             flip(s, k)
+    take_near(0, 0)
+    when_inner((relay, 0, 0), (to_end, 0, 1))
+    near_rows(0)
+    forward_all(0, 0, first)
+    far_rows(0)
+    when_inner((take_near, 0, 1), (relay, 0, 1), (to_inner, 0, 2), (to_end, 0, 2))
+    forward_all(0, 0, second)
+    when_end((take_near, 0, 1))
+    forward_all(0, 1, first)
+    collect(0, 0)
+    when_end(*[(send_both, 1, k) for k in range(MATS)], (send_both, 2, 0), (send_both, 2, 1))
+    gate_rows(0, 0)
+    forward_all(0, 1, second)
+    send_own(0, 2)
+    take_near(0, 2)
+    when_inner((relay, 0, 2))
+    when_inner(*[(act, 1, k) for k in range(MATS) for act in (send_near, to_inner, to_end, relay)])
+    collect(0, 1)
+    when_inner(*[(take_near, 1, k) for k in range(MATS)])
+    when_inner((send_near, 2, 0), (send_near, 2, 1), (to_inner, 2, 0), (to_inner, 2, 1))
+    hidden_rows(0, 0)
+    reduce_rows(0, 0, hid, [1], True)
+    when_end(*[(take_near, 1, k) for k in range(MATS)])
     for k in range(MATS):
         send_own(1, k)
     send_own(2, 0)
-    forward_all(0, 0, [1])
-    when_inner((relay, 0, 0), (send_cross, 0, 2))
-    near_rows(0)
-    forward_all(0, 0, first)
-    far_rows(0)
-    forward_all(0, 0, second)
-    forward_all(0, 1, [1])
-    when_inner((relay, 0, 1), (send_near, 2, 0))
-    collect(0, 0)
-    when_end(*[(send_both, 1, k) for k in range(MATS)], (send_both, 2, 0), (send_both, 2, 1))
-    gate_rows(0, 0)
-    forward_all(0, 1, first)
-    forward_all(0, 2, [1])
-    when_inner((relay, 0, 2))
-    forward_all(0, 1, second)
-    when_inner(*[(act, 1, k) for k in range(MATS) for act in (send_near, send_cross, relay)])
-    collect(0, 1)
-    for k in range(MATS):
-        forward_all(1, k, [1])
-    when_inner((send_near, 2, 1))
-    hidden_rows(0, 0)
-    reduce_rows(0, 0, hid, [1], True)
-    when_inner((send_cross, 2, 0), (send_cross, 2, 1), (send_cross, 2, 2))
     for f in range(n):
         res[f] = (tokens[f].astype(jnp.float32) + 0.5 * reduced(0, f)).astype(jnp.bfloat16)
     send_rows(1, lambda f: res[f].astype(jnp.float32), gainm)
     when_end((send_both, 2, 2))
     for k in range(MATS):
         forward_all(1, k, range(2, nz))
-    forward_all(2, 0, [1])
-    when_inner((relay, 2, 0), (relay, 2, 1))
+    when_end((take_near, 2, 0), (take_near, 2, 1))
     near_rows(1)
+    when_inner((to_end, 2, 0), (take_near, 2, 0), (to_end, 2, 1), (take_near, 2, 1))
+    when_inner((relay, 2, 0), (relay, 2, 1), (to_inner, 2, 2))
     when_inner((send_near, 2, 2))
     send_own(2, 1)
     far_rows(1)
     for k in range(MATS - 1):
         collect(1, k)
-    forward_all(2, 1, [1])
     mix_rows(1, 1)
     forward_all(2, 0, first)
-    send_own(2, 2)
     drain(0)
     reduce_rows(1, 1, hid_m, range(1, nz))
-    forward_all(2, 2, [1])
-    when_inner((relay, 2, 2))
     forward_all(2, 1, first)
     for f in range(n):
         res[f] = (res[f].astype(jnp.float32) + reduced(1, f)).astype(jnp.bfloat16)
     send_rows(2, lambda f: res[f].astype(jnp.float32), gain2)
-    forward_all(2, 2, first)
     forward_all(2, 0, second)
     near_rows(2)
+    when_inner((to_end, 2, 2), (relay, 2, 2))
+    take_near(2, 2)
+    forward_all(2, 1, second)
+    send_own(2, 2)
     far_rows(2)
-    forward_all(2, 1, second)
     collect(2, 0)
     gate_rows(2, 2)
     collect(2, 1)
-    hidden_rows(2, 2)
+    hidden_rows(2, 2, first)
     drain(1)
     reduce_rows(2, 2, hid, [1, *first], True)
     for f in range(n):

time: 272 us -> 259 us (0.952)
  Pallas kernels: 268 us -> 256 us
    pallas_call x1, Pallas kernels: 268 us -> 256 us  [body(): pl.pallas_call(functools.partial(layer_kernel, n, t), out_shape=jax.Shape...]
where the time goes in v2:
time: 259 us
  Pallas kernels  256 us (99%)
  local copies, waits for them, and re-layouts  3.03 us (1%)
    pallas_call x1, Pallas kernels, body(): pl.pallas_call(functools.partial(layer_kernel, n, t), out_shape=jax.Shape...  256 us

profile of v2, /device:TPU:0, one launch (start us, length us, event | category | flops | bytes accessed | tf_op | source)
XLA Modules:
  0.0 258.6 jit_solution(6622352410173917545)
XLA Ops:
  0.0 0.0 copy-start
  0.0 0.7 copy-done
  0.7 0.6 broadcast_in_dim.15.refs_7_
  1.3 255.5 %shard_map.163 = bf16[8,96,256]{2,1,0:T(8,128)(2,1)} custom-call(bf16[96,2048]{1,0:T(8,128)(2,1)} %refs_0_.1, f32[1,2048]{1,0:T(1,128)} %bitcast.13, f32[1,2048]{1,0:T(1,128)} %bitcast.14, f32[1,2048]{1,0:T(1,128)} %bitcast.15, bf16[4,384]{1,0:T(4,128)(2,1)} %refs_4_.1, bf16[6,64,64]{2,1,0:T(8,128)(2,1)} %refs_5_.1, bf16[6,64,64]{2,1,0:T(8,128)(2,1)} %refs_6_.1, ...), custom_call_target="tpu_custom_call" | custom-call | tf_op jit(solution)/shard_map/pallas_call | solution.py:657
  256.8 1.8 copy.19
  (1 shorter events, 0.0 us)
Async XLA Ops:
  0.0 0.7 copy-start

commit v3 on v2

--- a/solution.py
+++ b/solution.py
@@ -13,6 +13,7 @@
 PAIR = 2
 MATS = 3
 ROW_PARTS = 4
+LANES = 128
 MESH = pl.DeviceIdType.MESH
 
 
@@ -105,6 +106,7 @@
     chips, nx, ny, nz = me.chips, me.nx, me.ny, me.nz
     parts = math.gcd(n, ROW_PARTS)
     step = n // parts
+    group = 1 if dn % LANES else math.gcd(n, 4)
     mine = me.zp * nx + me.x
     rest = (1 - me.zp) * nx + me.x
 
@@ -364,12 +366,13 @@
     def project(g, s, k, c, to):
         acc[to] = jnp.zeros_like(acc[to])
 
-        def feature(f, carry):
-            rows = rows_of[g, :, c, f].reshape(chips * r, dn)
-            acc[to] += dot_nt(rows, weights[s][k, f])
+        def feature(m, carry):
+            rows = [rows_of[g, :, c, m * group + d].reshape(chips * r, dn) for d in range(group)]
+            units = [weights[s][k, m * group + d] for d in range(group)]
+            acc[to] += dot_nt(jnp.concatenate(rows, axis=1), jnp.concatenate(units, axis=1))
             return carry
 
-        lax.fori_loop(0, n, feature, 0)
+        lax.fori_loop(0, n // group, feature, 0)
 
     def gate_rows(g, s):
         def side(c, carry):
@@ -511,8 +514,9 @@
     forward_all(2, 0, second)
     near_rows(2)
     when_inner((to_end, 2, 2), (relay, 2, 2))
-    take_near(2, 2)
+    when_inner((take_near, 2, 2))
     forward_all(2, 1, second)
+    when_end((take_near, 2, 2))
     send_own(2, 2)
     far_rows(2)
     collect(2, 0)

time: 259 us -> 256 us (0.988)
  Pallas kernels: 256 us -> 251 us
    pallas_call x1, Pallas kernels: 256 us -> 251 us  [body(): pl.pallas_call(functools.partial(layer_kernel, n, t), out_shape=jax.Shape...]
where the time goes in v3:
time: 256 us; the launch traced here: 254 us
  Pallas kernels  251 us (98%)
  local copies, waits for them, and re-layouts  3.03 us (1%)
    pallas_call x1, Pallas kernels, body(): pl.pallas_call(functools.partial(layer_kernel, n, t), out_shape=jax.Shape...  251 us

profile of v3, /device:TPU:0, one launch (start us, length us, event | category | flops | bytes accessed | tf_op | source)
XLA Modules:
  0.0 253.9 jit_solution(11893280338618117531)
XLA Ops:
  0.0 0.0 copy-start
  0.0 0.7 copy-done
  0.7 0.6 broadcast_in_dim.15.refs_7_
  1.3 250.8 %shard_map.163 = bf16[8,96,256]{2,1,0:T(8,128)(2,1)} custom-call(bf16[96,2048]{1,0:T(8,128)(2,1)} %refs_0_.1, f32[1,2048]{1,0:T(1,128)} %bitcast.13, f32[1,2048]{1,0:T(1,128)} %bitcast.14, f32[1,2048]{1,0:T(1,128)} %bitcast.15, bf16[4,384]{1,0:T(4,128)(2,1)} %refs_4_.1, bf16[6,64,64]{2,1,0:T(8,128)(2,1)} %refs_5_.1, bf16[6,64,64]{2,1,0:T(8,128)(2,1)} %refs_6_.1, ...), custom_call_target="tpu_custom_call" | custom-call | tf_op jit(solution)/shard_map/pallas_call | solution.py:661
  252.1 1.8 copy.19
  (1 shorter events, 0.0 us)
Async XLA Ops:
  0.0 0.7 copy-start
